TPU v7x, 32 devices: a whole 2x2x4 slice. The times are simulated.
32 devices in a mesh: fs: 8 (over z, core), tp: 4 (over y, x).
Axes of the slice: x: 2, y: 2, z: 4, core: 2. Of those that a mesh axis runs over, the one named last changes fastest.
Arguments:
- in_saved: bfloat16 [6144, 2048], P(('fs', 'tp')), may hold values from -6 to 6
- in_cotangent: bfloat16 [6144, 2048], P(('fs', 'tp')), as said below
- point_saved: bfloat16 [6144, 2048], P(('fs', 'tp')), may hold values from -6 to 6
- point_cotangent: bfloat16 [6144, 2048], P(('fs', 'tp')), as said below
- in_basis: bfloat16 [2048, 128], replicated, as said below
- point_basis: bfloat16 [2048, 128], replicated, as said below
- in_first: float32 [128, 2048], P('fs', 'tp'), may hold values from -3 to 3
- in_second: float32 [128, 2048], P('fs', 'tp'), may hold values from 0.02 to 2
- point_first: float32 [128, 2048], P('fs', 'tp'), may hold values from -3 to 3
- point_second: float32 [128, 2048], P('fs', 'tp'), may hold values from 0.02 to 2
- in_master: float32 [2048, 2048], P('fs', 'tp'), may hold values from -3 to 3
- point_master: float32 [2048, 2048], P('fs', 'tp'), may hold values from -3 to 3
Outputs:
- in_first_new: float32 [128, 2048], P('fs', 'tp')
- in_second_new: float32 [128, 2048], P('fs', 'tp')
- point_first_new: float32 [128, 2048], P('fs', 'tp')
- point_second_new: float32 [128, 2048], P('fs', 'tp')
- in_step: float32 [2048, 2048], P('fs', 'tp')
- point_step: float32 [2048, 2048], P('fs', 'tp')
- in_master_new: float32 [2048, 2048], P('fs', 'tp')
- point_master_new: float32 [2048, 2048], P('fs', 'tp')
- in_copy: bfloat16 [2048, 2048], P(None, 'tp')
- point_copy: bfloat16 [2048, 2048], P(None, 'tp')
Inputs may be any that keep to these rules, and one draw needn't show every extreme that they name: `in_cotangent`: real-valued entries of every column. `point_cotangent`: real-valued entries of every column. `in_basis`: real-valued basis of full rank. `point_basis`: real-valued basis of full rank.
All inputs are finite; a program needn't handle non-finite values.
Results may differ from a plain program's by a relative error of at most 0.0034.
Values may be sent and summed in bfloat16 or wider, within the bound.
A program may use at most 64 MiB of HBM per device.

v0:
```python
import jax
import jax.numpy as jnp
from jax import lax
from jax.sharding import PartitionSpec as P


def low_term(saved, cotangent, basis):
    reduced = jnp.dot(saved, basis, preferred_element_type=jnp.float32).astype(jnp.bfloat16)
    return lax.dot_general(
        reduced, cotangent, (((0,), (0,)), ((), ())), preferred_element_type=jnp.float32
    )


def moments(first, second, grad):
    first_new = 0.8 * first + 0.2 * grad
    second_new = 0.9 * second + 0.1 * grad * grad
    return (first_new, second_new, first_new / (jnp.sqrt(second_new) + 1e-08))


def weight_step(basis, direction, fs_count):
    row_count = basis.shape[0] // fs_count
    rows_here = lax.dynamic_slice_in_dim(basis, lax.axis_index("fs") * row_count, row_count, 0)
    return -jnp.dot(rows_here.astype(jnp.float32), direction, precision=lax.Precision.HIGHEST)


def body(
    in_saved,
    in_cotangent,
    point_saved,
    point_cotangent,
    in_basis,
    point_basis,
    in_first,
    in_second,
    point_first,
    point_second,
    in_master,
    point_master,
):
    fs_count = lax.axis_size("fs")
    in_low = low_term(in_saved, in_cotangent, in_basis)
    point_low = low_term(point_saved, point_cotangent, point_basis)
    rank_rows = in_low.shape[0]
    entries = 1.0 * rank_rows * (in_low.shape[1] + point_low.shape[1])
    part_in, part_point = (
        lax.psum_scatter(in_low, "tp", scatter_dimension=1, tiled=True),
        lax.psum_scatter(point_low, "tp", scatter_dimension=1, tiled=True),
    )
    sum_in, sum_point = lax.psum((part_in, part_point), "fs")
    squares = lax.psum(jnp.sum(sum_in * sum_in) + jnp.sum(sum_point * sum_point), "tp")
    clip_factor = jnp.minimum(1.0, 1.0 / jnp.sqrt(squares / entries + 1e-06))
    previous = (
        lax.all_gather(in_first, "fs", axis=0, tiled=True),
        lax.all_gather(in_second, "fs", axis=0, tiled=True),
        lax.all_gather(point_first, "fs", axis=0, tiled=True),
        lax.all_gather(point_second, "fs", axis=0, tiled=True),
    )
    in_first_all, in_second_all, in_direction = moments(
        previous[0], previous[1], clip_factor * sum_in
    )
    point_first_all, point_second_all, point_direction = moments(
        previous[2], previous[3], clip_factor * sum_point
    )
    row_count = rank_rows // fs_count
    row_start = lax.axis_index("fs") * row_count
    in_first_new = lax.dynamic_slice_in_dim(in_first_all, row_start, row_count, 0)
    in_second_new = lax.dynamic_slice_in_dim(in_second_all, row_start, row_count, 0)
    point_first_new = lax.dynamic_slice_in_dim(point_first_all, row_start, row_count, 0)
    point_second_new = lax.dynamic_slice_in_dim(point_second_all, row_start, row_count, 0)
    in_step = weight_step(in_basis, in_direction, fs_count)
    point_step = weight_step(point_basis, point_direction, fs_count)
    in_master_new = in_master + in_step
    point_master_new = point_master + point_step
    in_copy, point_copy = (
        lax.all_gather(in_master_new.astype(jnp.bfloat16), "fs", axis=0, tiled=True),
        lax.all_gather(point_master_new.astype(jnp.bfloat16), "fs", axis=0, tiled=True),
    )
    return (
        in_first_new,
        in_second_new,
        point_first_new,
        point_second_new,
        in_step,
        point_step,
        in_master_new,
        point_master_new,
        in_copy,
        point_copy,
    )


def solution(mesh):
    return jax.shard_map(
        body,
        mesh=mesh,
        in_specs=(
            P(("fs", "tp"), None),
            P(("fs", "tp"), None),
            P(("fs", "tp"), None),
            P(("fs", "tp"), None),
            P(),
            P(),
            P("fs", "tp"),
            P("fs", "tp"),
            P("fs", "tp"),
            P("fs", "tp"),
            P("fs", "tp"),
            P("fs", "tp"),
        ),
        out_specs=(
            P("fs", "tp"),
            P("fs", "tp"),
            P("fs", "tp"),
            P("fs", "tp"),
            P("fs", "tp"),
            P("fs", "tp"),
            P("fs", "tp"),
            P("fs", "tp"),
            P(None, "tp"),
            P(None, "tp"),
        ),
        check_vma=False,
    )
```

profile of v0, /device:TPU:0, one launch (start us, length us, event | category | flops | bytes accessed | tf_op | source)
XLA Modules:
  0.0 221.0 jit_solution(17097462439443650107)
XLA Ops:
  7.2 0.0 copy-start
  7.2 0.0 copy-start.4
  7.2 0.0 copy-start.2
  7.2 0.0 copy-start.3
  7.2 0.0 reduce-scatter.3.cloned.1.call-start
  7.3 1.0 copy-done
  8.3 2.9 %fusion = f32[128,2048]{1,0:T(8,128)} fusion(bf16[192,2048]{1,0:T(8,128)(2,1)S(1)} %copy-done, bf16[192,2048]{1,0:T(8,128)(2,1)} %param.12, bf16[2048,128]{1,0:T(8,128)(2,1)} %param.16), kind=kOutput, calls=%fused_computation.4 | convolution fusion | flops 201351168 | bytes 3145728 | tf_op jit(solution)/shard_map/dot_general | solution.py:9
  11.2 0.0 reduce-scatter.3.cloned.1.call-update
  11.3 0.0 copy-start.6
  11.3 0.0 copy-start.7
  11.3 0.0 copy-start.8
  11.3 0.0 copy-start.9
  11.3 0.0 reduce-scatter.5.cloned.1.call-start
  11.4 0.0 copy-done.4
  11.4 0.0 copy-done.2
  11.4 0.0 copy-done.3
  11.4 1.6 fusion.1
  13.0 0.0 reduce-scatter.5.cloned.1.call-update
  13.1 0.0 all-reduce.3.cloned.1.call-start
  13.1 0.0 copy-done.6
  13.1 15.9 %all_gather.18 = f32[128,512]{1,0:T(8,128)S(1)} all-gather(f32[16,512]{1,0:T(8,128)S(1)} %copy-done.6), channel_id=1, replica_groups=mesh['fs'=8,'tp'=4] {'fs'}, dimensions={0}, use_global_device_ids=true | all-gather | bytes 294912 | tf_op jit(solution)/shard_map/all_gather | solution.py:53
  29.0 13.2 %reduce-scatter.3.cloned.1.call-done = f32[128,512]{1,0:T(8,128)} async-done(((f32[128,2048]{1,0:T(8,128)}), f32[128,512]{1,0:T(8,128)}) %reduce-scatter.3.cloned.1.call-update) | async-done | bytes 262160 | tf_op jit(solution)/shard_map/reduce_scatter | solution.py:46
  42.2 31.4 %reduce-scatter.5.cloned.1.call-done = f32[128,512]{1,0:T(8,128)} async-done(((f32[128,2048]{1,0:T(8,128)}), f32[128,512]{1,0:T(8,128)}) %reduce-scatter.5.cloned.1.call-update) | async-done | bytes 262160 | tf_op jit(solution)/shard_map/reduce_scatter | solution.py:47
  73.6 0.0 all-reduce.3.cloned.1.call-update
  73.6 0.0 all-gather.5.cloned.1.call-start
  73.7 0.0 copy-done.7
  73.7 14.4 %all_gather.19 = f32[128,512]{1,0:T(8,128)S(1)} all-gather(f32[16,512]{1,0:T(8,128)S(1)} %copy-done.7), channel_id=1, replica_groups=mesh['fs'=8,'tp'=4] {'fs'}, dimensions={0}, use_global_device_ids=true | all-gather | bytes 294912 | tf_op jit(solution)/shard_map/all_gather | solution.py:54
  88.1 0.0 copy-done.8
  88.1 14.5 %all_gather.20 = f32[128,512]{1,0:T(8,128)S(1)} all-gather(f32[16,512]{1,0:T(8,128)S(1)} %copy-done.8), channel_id=1, replica_groups=mesh['fs'=8,'tp'=4] {'fs'}, dimensions={0}, use_global_device_ids=true | all-gather | bytes 294912 | tf_op jit(solution)/shard_map/all_gather | solution.py:55
  102.6 0.0 copy-done.9
  102.6 14.4 %all_gather.21 = f32[128,512]{1,0:T(8,128)S(1)} all-gather(f32[16,512]{1,0:T(8,128)S(1)} %copy-done.9), channel_id=1, replica_groups=mesh['fs'=8,'tp'=4] {'fs'}, dimensions={0}, use_global_device_ids=true | all-gather | bytes 294912 | tf_op jit(solution)/shard_map/all_gather | solution.py:56
  117.1 16.2 %all-reduce.3.cloned.1.call-done = (f32[128,512]{1,0:T(8,128)}, f32[128,512]{1,0:T(8,128)}) async-done(((f32[128,512]{1,0:T(8,128)}, f32[128,512]{1,0:T(8,128)}), (f32[128,512]{1,0:T(8,128)}, f32[128,512]{1,0:T(8,128)})) %all-reduce.3.cloned.1.call-update) | async-done | bytes 524304 | tf_op jit(solution)/shard_map/psum | solution.py:49
  133.3 1.6 multiply_reduce_fusion
  134.9 1.6 multiply_reduce_fusion.1
  137.8 10.2 %psum.23 = f32[]{:T(128)} all-reduce(f32[]{:T(128)S(6)} %add.50), channel_id=1, replica_groups=mesh['fs'=8,'tp'=4] {'tp'}, use_global_device_ids=true, to_apply=%region_6.0 | all-reduce | flops 1 | bytes 8 | tf_op jit(solution)/shard_map/psum | solution.py:50
  148.7 1.2 fusion.2
  149.9 0.0 copy-start.5
  150.0 2.7 %fusion.18 = (bf16[256,512]{1,0:T(8,128)(2,1)}, f32[256,512]{1,0:T(8,128)}, f32[256,512]{1,0:T(8,128)}) fusion(f32[256,512]{1,0:T(8,128)} %param.23, f32[128,512]{1,0:T(8,128)S(1)} %get-tuple-element.22, f32[128,512]{1,0:T(8,128)S(1)} %get-tuple-element.23, bf16[2048,128]{1,0:T(8,128)(2,1)S(1)} %copy-done.4, s32[]{:T(128)S(6)} %select_n.5), kind=kOutput, calls=%fused_computation.32 | convolution fusion | flops 201850880 | bytes 2424836 | tf_op jit(solution)/shard_map/dot_general | solution.py:23
  152.6 0.0 all-gather.5.cloned.1.call-update
  152.6 0.0 all-gather.3.cloned.1.call-start
  152.7 0.0 copy-done.5
  152.7 2.4 %fusion.19 = (bf16[256,512]{1,0:T(8,128)(2,1)}, f32[256,512]{1,0:T(8,128)}, f32[256,512]{1,0:T(8,128)}) fusion(f32[256,512]{1,0:T(8,128)S(1)} %copy-done.5, f32[128,512]{1,0:T(8,128)S(1)} %get-tuple-element.19, f32[128,512]{1,0:T(8,128)S(1)} %get-tuple-element.18, bf16[2048,128]{1,0:T(8,128)(2,1)} %param.16, s32[]{:T(128)S(6)} %select_n.5), kind=kOutput, calls=%fused_computation.33 | convolution fusion | flops 201850880 | bytes 2424836 | tf_op jit(solution)/shard_map/dot_general | solution.py:23
  155.1 0.0 all-gather.3.cloned.1.call-update
  155.1 0.6 constant_dynamic-slice_fusion.2
  155.8 0.6 constant_dynamic-slice_fusion.3
  156.4 0.6 constant_dynamic-slice_fusion.1
  157.0 0.6 constant_dynamic-slice_fusion
  157.6 21.7 %all-gather.5.cloned.1.call-done = bf16[2048,512]{1,0:T(8,128)(2,1)} async-done(((bf16[256,512]{1,0:T(8,128)(2,1)}), bf16[2048,512]{1,0:T(8,128)(2,1)}) %all-gather.5.cloned.1.call-update) | async-done | bytes 2097168 | tf_op jit(solution)/shard_map/all_gather | solution.py:76
  179.3 30.6 %all-gather.3.cloned.1.call-done = bf16[2048,512]{1,0:T(8,128)(2,1)} async-done(((bf16[256,512]{1,0:T(8,128)(2,1)}), bf16[2048,512]{1,0:T(8,128)(2,1)}) %all-gather.3.cloned.1.call-update) | async-done | bytes 2097168 | tf_op jit(solution)/shard_map/all_gather | solution.py:75
  209.9 0.0 copy-start.1
  209.9 3.2 %copy.26 = bf16[2048,512]{1,0:T(8,128)(2,1)} copy(bf16[2048,512]{1,0:T(8,128)(2,1)} %all-gather.3.cloned.1.call-done) | data formatting | bytes 4194304
  213.1 0.0 copy-done.1
  213.1 1.3 copy.27
Async XLA Ops:
  7.2 1.1 copy-start
  7.2 4.2 %copy-start.4 = (bf16[2048,128]{1,0:T(8,128)(2,1)S(1)}, bf16[2048,128]{1,0:T(8,128)(2,1)}, u32[]{:S(2)}) copy-start(bf16[2048,128]{1,0:T(8,128)(2,1)} %param.17) | copy-start | bytes 1572868
  7.2 4.2 %copy-start.2 = (bf16[192,2048]{1,0:T(8,128)(2,1)S(1)}, bf16[192,2048]{1,0:T(8,128)(2,1)}, u32[]{:S(2)}) copy-start(bf16[192,2048]{1,0:T(8,128)(2,1)} %param.15) | copy-start | bytes 2359300
  7.2 4.2 %copy-start.3 = (bf16[192,2048]{1,0:T(8,128)(2,1)S(1)}, bf16[192,2048]{1,0:T(8,128)(2,1)}, u32[]{:S(2)}) copy-start(bf16[192,2048]{1,0:T(8,128)(2,1)} %param.14) | copy-start | bytes 2359300
  7.2 35.0 %reduce-scatter.3.cloned.1.call-start = ((), (), s32[]{:S(2)}) async-start(), calls=%async_computation.2 | async-start | bytes 1310720 | tf_op jit(solution)/shard_map/reduce_scatter | solution.py:46
  11.3 1.9 copy-start.6
  11.3 62.4 %copy-start.7 = (f32[16,512]{1,0:T(8,128)S(1)}, f32[16,512]{1,0:T(8,128)}, u32[]{:S(2)}) copy-start(f32[16,512]{1,0:T(8,128)} %param.19) | copy-start | bytes 98308
  11.3 76.8 %copy-start.8 = (f32[16,512]{1,0:T(8,128)S(1)}, f32[16,512]{1,0:T(8,128)}, u32[]{:S(2)}) copy-start(f32[16,512]{1,0:T(8,128)} %param.20) | copy-start | bytes 98308
  11.3 91.3 %copy-start.9 = (f32[16,512]{1,0:T(8,128)S(1)}, f32[16,512]{1,0:T(8,128)}, u32[]{:S(2)}) copy-start(f32[16,512]{1,0:T(8,128)} %param.21) | copy-start | bytes 98308
  11.3 62.3 %reduce-scatter.5.cloned.1.call-start = ((), (), s32[]{:S(2)}) async-start(), calls=%async_computation.3 | async-start | bytes 1310720 | tf_op jit(solution)/shard_map/reduce_scatter | solution.py:47
  13.1 120.2 %all-reduce.3.cloned.1.call-start = ((), (), s32[]{:S(2)}) async-start(), calls=%async_computation.6 | async-start | bytes 1048576 | tf_op jit(solution)/shard_map/psum | solution.py:49
  73.6 105.7 %all-gather.5.cloned.1.call-start = ((), (), s32[]{:S(2)}) async-start(), calls=%async_computation.5 | async-start | bytes 2359296 | tf_op jit(solution)/shard_map/all_gather | solution.py:76
  149.9 2.8 %copy-start.5 = (f32[256,512]{1,0:T(8,128)S(1)}, f32[256,512]{1,0:T(8,128)}, u32[]{:S(2)}) copy-start(f32[256,512]{1,0:T(8,128)} %param.22) | copy-start | bytes 1572868
  152.6 57.3 %all-gather.3.cloned.1.call-start = ((), (), s32[]{:S(2)}) async-start(), calls=%async_computation.4 | async-start | bytes 2359296 | tf_op jit(solution)/shard_map/all_gather | solution.py:75
  209.9 3.2 %copy-start.1 = (bf16[2048,512]{1,0:T(8,128)(2,1)S(1)}, bf16[2048,512]{1,0:T(8,128)(2,1)}, u32[]{:S(2)}) copy-start(bf16[2048,512]{1,0:T(8,128)(2,1)} %all-gather.5.cloned.1.call-done) | copy-start | bytes 6291460
Sparse Core Ops, SparseCore 0:
  11.5 30.6 reduce-scatter.2
  45.7 27.9 reduce-scatter.4
  76.0 57.2 all-reduce.2
  152.8 26.5 all-gather.4
  181.4 28.5 all-gather.2
where the time goes:
time: 221 us
  waiting for transfers between devices  113 us (51%)
  blocking collectives  69.4 us (31%)
  between operations  15.9 us (7%)
  matrix products  9.64 us (4%)
  local copies, waits for them, and re-layouts  8.09 us (4%)
  other arithmetic  4.47 us (2%)
    reduce_scatter x1, waiting for transfers between devices, body(): lax.psum_scatter(point_low, 'tp', scatter_dimension=1, tiled=True)  31.4 us
    all_gather x1, waiting for transfers between devices, body(): lax.all_gather(in_master_new.astype(jnp.bfloat16), 'fs', axis=0, tiled=True)  30.6 us
    all_gather x1, waiting for transfers between devices, body(): lax.all_gather(point_master_new.astype(jnp.bfloat16), 'fs', axis=0, tiled...  21.7 us
    psum x1, waiting for transfers between devices, body(): sum_in, sum_point = lax.psum((part_in, part_point), 'fs')  16.2 us
    all_gather x1, blocking collectives, body(): lax.all_gather(in_first, 'fs', axis=0, tiled=True)  15.9 us
    all_gather x1, blocking collectives, body(): lax.all_gather(point_first, 'fs', axis=0, tiled=True)  14.5 us
    all_gather x1, blocking collectives, body(): lax.all_gather(point_second, 'fs', axis=0, tiled=True)  14.4 us
    all_gather x1, blocking collectives, body(): lax.all_gather(in_second, 'fs', axis=0, tiled=True)  14.4 us
  transfers between devices with their start and end apart: 5, of which 5 were waited for; matrix products, arithmetic and copies ran while one was open for 3% of the time, Pallas kernels for 0%

commit v1 on v0

--- a/solution.py
+++ b/solution.py
@@ -1,6 +1,10 @@
+import functools
+
 import jax
 import jax.numpy as jnp
 from jax import lax
+from jax.experimental import pallas as pl
+from jax.experimental.pallas import tpu as pltpu
 from jax.sharding import PartitionSpec as P
 
 
@@ -89,9 +93,444 @@
     )
 
 
+MESH = pl.DeviceIdType.MESH
+HBM = pl.BlockSpec(memory_space=pl.ANY)
+WHOLE = pl.BlockSpec(memory_space=pltpu.VMEM)
+
+
+def exchange_kernel(
+    n_fs,
+    n_tp,
+    in_saved,
+    in_cot,
+    point_saved,
+    point_cot,
+    in_basis,
+    point_basis,
+    in_first,
+    in_second,
+    point_first,
+    point_second,
+    in_master,
+    point_master,
+    dirs_out,
+    moments_out,
+    gathered_out,
+    saved,
+    cot,
+    basis,
+    master,
+    part,
+    mate,
+    tp_got,
+    fs_got,
+    total,
+    dirs,
+    gathered,
+    scalars,
+    load_sem,
+    out_sem,
+    mate_sems,
+    tp_sems,
+    fs_sems,
+    tp_scalar_sems,
+    fs_scalar_sems,
+    dir_sems,
+    dir_mate_sems,
+    ring_sems,
+    ring_mate_sems,
+):
+    f, t = lax.axis_index("fs"), lax.axis_index("tp")
+    z, core = f // 2, f % 2
+    n_z = n_fs // 2
+    mate_f = f + 1 - 2 * core
+    width = in_first.shape[1]
+    rows = in_first.shape[0]
+
+    def at_z(step):
+        return lax.rem(z + step + n_z, n_z)
+
+    def at_tp(step):
+        return lax.rem(t + step + n_tp, n_tp)
+
+    def at_fs(step):
+        return lax.rem(f + step + n_fs, n_fs)
+
+    def remote(src, dst, sems, index, device):
+        return pltpu.make_async_remote_copy(
+            src_ref=src,
+            dst_ref=dst,
+            send_sem=sems.at[(0, *index)],
+            recv_sem=sems.at[(1, *index)],
+            device_id=device,
+            device_id_type=MESH,
+        )
+
+    loads = []
+    sources = (
+        (in_master, master.at[0]),
+        (point_master, master.at[1]),
+        (in_basis, basis.at[0]),
+        (in_saved, saved.at[0]),
+        (in_cot, cot.at[0]),
+        (point_basis, basis.at[1]),
+        (point_saved, saved.at[1]),
+        (point_cot, cot.at[1]),
+    )
+    for k, (src, dst) in enumerate(sources):
+        copy = pltpu.make_async_copy(src, dst, load_sem.at[k])
+        copy.start()
+        loads.append(copy)
+
+    barrier = pltpu.get_barrier_semaphore()
+    for step in range(1, n_fs):
+        pl.semaphore_signal(barrier, inc=1, device_id=(at_fs(step), t), device_id_type=MESH)
+    for step in range(1, n_tp):
+        pl.semaphore_signal(barrier, inc=1, device_id=(f, at_tp(step)), device_id_type=MESH)
+
+    sends = []
+    outs = []
+
+    def put_out(m, order, slot):
+        copy = pltpu.make_async_copy(
+            gathered.at[m, slot], gathered_out.at[m, slot], out_sem.at[m, order]
+        )
+        copy.start()
+        outs.append(copy)
+
+    def ring_send(step):
+        for m in range(2):
+            slot = 2 * at_z(-step if m == 0 else step) + core
+            copy = remote(
+                gathered.at[m, slot],
+                gathered.at[m, slot],
+                ring_sems,
+                (m, step),
+                (2 * at_z(1 if m == 0 else -1) + core, t),
+            )
+            copy.start()
+            sends.append(copy)
+
+    def mate_send(step):
+        for m in range(2):
+            slot = 2 * at_z(-step if m == 0 else step) + core
+            copy = remote(
+                gathered.at[m, slot], gathered.at[m, slot], ring_mate_sems, (m, step), (mate_f, t)
+            )
+            copy.start()
+            sends.append(copy)
+            put_out(m, step, slot)
+
+    def ring_wait(step):
+        for m in range(2):
+            slot = 2 * at_z(-step - 1 if m == 0 else step + 1) + core
+            remote(
+                gathered.at[m, slot], gathered.at[m, slot], ring_sems, (m, step), (f, t)
+            ).wait_recv()
+
+    def ring_advance(step):
+        ring_wait(step - 1)
+        if step < n_z - 1:
+            ring_send(step)
+        mate_send(step)
+
+    for m in range(2):
+        loads[m].wait()
+        gathered[m, f] = master[m].astype(jnp.bfloat16)
+    pl.semaphore_wait(barrier, n_fs + n_tp - 2)
+    ring_send(0)
+    mate_send(0)
+
+    for m in range(2):
+        for k in range(3):
+            loads[2 + 3 * m + k].wait()
+        reduced = jnp.dot(saved[m], basis[m], preferred_element_type=jnp.float32).astype(
+            jnp.bfloat16
+        )
+        for k in range(n_tp):
+            low = lax.dot_general(
+                reduced,
+                cot[m, :, k * width : (k + 1) * width],
+                (((0,), (0,)), ((), ())),
+                preferred_element_type=jnp.float32,
+            )
+            for g in range(n_fs):
+                part[m, g % 2, k, g // 2] = low[g * rows : (g + 1) * rows]
+        copy = remote(part.at[m, 1 - core], mate.at[m], mate_sems, (m,), (mate_f, t))
+        copy.start()
+        sends.append(copy)
+
+    for m in range(2):
+        remote(mate.at[m], mate.at[m], mate_sems, (m,), (mate_f, t)).wait_recv()
+        for step in range(1, n_tp + 1):
+            to = at_tp(step) if step < n_tp else t
+            part[m, core, to] = part[m, core, to] + mate[m, to]
+            if step < n_tp:
+                copy = remote(
+                    part.at[m, core, to], tp_got.at[m, step - 1], tp_sems, (m, step - 1), (f, to)
+                )
+                copy.start()
+                sends.append(copy)
+    ring_advance(1)
+
+    for m in range(2):
+        for step in range(1, n_tp):
+            remote(
+                tp_got.at[m, step - 1], tp_got.at[m, step - 1], tp_sems, (m, step - 1), (f, t)
+            ).wait_recv()
+        for step in range(1, n_z + 1):
+            to = at_z(step) if step < n_z else z
+            value = part[m, core, t, to]
+            for k in range(n_tp - 1):
+                value = value + tp_got[m, k, to]
+            total[m, to] = value
+            if step < n_z:
+                copy = remote(
+                    total.at[m, to],
+                    fs_got.at[m, step - 1],
+                    fs_sems,
+                    (m, step - 1),
+                    (2 * to + core, t),
+                )
+                copy.start()
+                sends.append(copy)
+    grads = []
+    for m in range(2):
+        value = total[m, z]
+        for step in range(1, n_z):
+            remote(
+                fs_got.at[m, step - 1], fs_got.at[m, step - 1], fs_sems, (m, step - 1), (f, t)
+            ).wait_recv()
+            value = value + fs_got[m, step - 1]
+        grads.append(value)
+
+    def add_scalars(value, count, base, sems, device):
+        scalars[base] = jnp.broadcast_to(value, scalars.shape[1:])
+        for step in range(1, count):
+            copy = remote(
+                scalars.at[base], scalars.at[base + step], sems, (step - 1,), device(step)
+            )
+            copy.start()
+            sends.append(copy)
+        result = scalars[base]
+        for step in range(1, count):
+            slot = scalars.at[base + step]
+            remote(slot, slot, sems, (step - 1,), (f, t)).wait_recv()
+            result = result + scalars[base + step]
+        return result[0:1, 0:1]
+
+    squares = jnp.sum(grads[0] * grads[0] + grads[1] * grads[1], keepdims=True)
+    squares = add_scalars(squares, n_tp, 0, tp_scalar_sems, lambda step: (f, at_tp(step)))
+    squares = add_scalars(squares, n_fs, n_tp, fs_scalar_sems, lambda step: (at_fs(step), t))
+    entries = 2.0 * rows * n_fs * width * n_tp
+    clip = jnp.minimum(1.0, 1.0 / jnp.sqrt(squares / entries + 1e-06))
+
+    old = ((in_first, in_second), (point_first, point_second))
+    for m in range(2):
+        first, second, direction = moments(old[m][0][...], old[m][1][...], clip * grads[m])
+        moments_out[2 * m] = first
+        moments_out[2 * m + 1] = second
+        dirs[f, m] = direction
+    for step in range(1, n_z):
+        copy = remote(
+            dirs.at[f], dirs.at[f], dir_sems, (step - 1,), (2 * at_z(step) + core, t)
+        )
+        copy.start()
+        sends.append(copy)
+
+    def dir_mate(step):
+        slot = 2 * at_z(-step) + core
+        copy = remote(dirs.at[slot], dirs.at[slot], dir_mate_sems, (step,), (mate_f, t))
+        copy.start()
+        sends.append(copy)
+
+    dir_mate(0)
+    for step in range(1, n_z):
+        slot = 2 * at_z(-step) + core
+        remote(dirs.at[slot], dirs.at[slot], dir_sems, (step - 1,), (f, t)).wait_recv()
+        dir_mate(step)
+    for step in range(2, n_z):
+        ring_advance(step)
+    for step in range(n_z):
+        slot = 2 * at_z(-step) + 1 - core
+        remote(dirs.at[slot], dirs.at[slot], dir_mate_sems, (step,), (f, t)).wait_recv()
+        for m in range(2):
+            slot = 2 * at_z(-step if m == 0 else step) + 1 - core
+            remote(
+                gathered.at[m, slot], gathered.at[m, slot], ring_mate_sems, (m, step), (f, t)
+            ).wait_recv()
+            put_out(m, n_z + step, slot)
+    dirs_out[...] = dirs[...]
+    for copy in sends:
+        copy.wait_send()
+    for copy in outs:
+        copy.wait()
+
+
+def exchange(n_fs, n_tp, *args):
+    saved, basis, first, master = args[0], args[4], args[6], args[10]
+    rows, width = first.shape
+    n_z = n_fs // 2
+    f32, bf16 = jnp.float32, jnp.bfloat16
+    dma = pltpu.SemaphoreType.DMA
+    return pl.pallas_call(
+        functools.partial(exchange_kernel, n_fs, n_tp),
+        out_shape=(
+            jax.ShapeDtypeStruct((n_fs, 2, rows, width), f32),
+            jax.ShapeDtypeStruct((4, rows, width), f32),
+            jax.ShapeDtypeStruct((2, n_fs, *master.shape), bf16),
+        ),
+        in_specs=[HBM] * 6 + [WHOLE] * 4 + [HBM] * 2,
+        out_specs=(WHOLE, WHOLE, HBM),
+        scratch_shapes=[
+            pltpu.VMEM((2, *saved.shape), bf16),
+            pltpu.VMEM((2, *args[1].shape), bf16),
+            pltpu.VMEM((2, *basis.shape), bf16),
+            pltpu.VMEM((2, *master.shape), f32),
+            pltpu.VMEM((2, 2, n_tp, n_z, rows, width), f32),
+            pltpu.VMEM((2, n_tp, n_z, rows, width), f32),
+            pltpu.VMEM((2, n_tp - 1, n_z, rows, width), f32),
+            pltpu.VMEM((2, n_z - 1, rows, width), f32),
+            pltpu.VMEM((2, n_z, rows, width), f32),
+            pltpu.VMEM((n_fs, 2, rows, width), f32),
+            pltpu.VMEM((2, n_fs, *master.shape), bf16),
+            pltpu.VMEM((n_tp + n_fs, 8, 128), f32),
+            dma((8,)),
+            dma((2, n_fs)),
+            dma((2, 2)),
+            dma((2, 2, n_tp - 1)),
+            dma((2, 2, n_z - 1)),
+            dma((2, n_tp - 1)),
+            dma((2, n_fs - 1)),
+            dma((2, n_z - 1)),
+            dma((2, n_z)),
+            dma((2, 2, n_z - 1)),
+            dma((2, 2, n_z)),
+        ],
+        compiler_params=pltpu.CompilerParams(
+            collective_id=0, has_side_effects=True, vmem_limit_bytes=48 * 2**20
+        ),
+        name="exchange",
+    )(*args)
+
+
+def update_kernel(
+    dirs,
+    moments_new,
+    in_basis,
+    point_basis,
+    in_gathered,
+    point_gathered,
+    in_master,
+    point_master,
+    in_first_new,
+    in_second_new,
+    point_first_new,
+    point_second_new,
+    in_step,
+    point_step,
+    in_master_new,
+    point_master_new,
+    in_copy,
+    point_copy,
+    split,
+):
+    i = pl.program_id(0)
+    f = lax.axis_index("fs")
+    rank = split.shape[1] // 2
+
+    @pl.when(i == 0)
+    def first_tile():
+        for m in range(2):
+            whole = dirs[:, m].reshape(rank, split.shape[2])
+            high = whole.astype(jnp.bfloat16)
+            split[m, :rank] = high
+            split[m, rank:] = (whole - high.astype(jnp.float32)).astype(jnp.bfloat16)
+        for k, out in enumerate(
+            (in_first_new, in_second_new, point_first_new, point_second_new)
+        ):
+            out[...] = moments_new[k]
+
+    groups = (
+        (in_basis, in_gathered, in_master, in_step, in_master_new, in_copy),
+        (point_basis, point_gathered, point_master, point_step, point_master_new, point_copy),
+    )
+    for m, (basis, gathered, master, step, master_new, copy) in enumerate(groups):
+        twice = jnp.concatenate([basis[...], basis[...]], axis=1)
+        move = -jnp.dot(twice, split[m], preferred_element_type=jnp.float32)
+        copy[...] = (gathered[0, 0].astype(jnp.float32) + move).astype(jnp.bfloat16)
+
+        @pl.when(i == f)
+        def own_tile():
+            step[...] = move
+            new = master[...] + move
+            master_new[...] = new
+            copy[...] = new.astype(jnp.bfloat16)
+
+
+def update(n_fs, dirs, moments_new, gathered, *args):
+    in_basis, in_first, in_master = args[4], args[6], args[10]
+    row_count, width = in_master.shape
+    rank = in_basis.shape[1]
+    f32, bf16 = jnp.float32, jnp.bfloat16
+
+    def fixed(shape):
+        return pl.BlockSpec(shape, lambda i: (0,) * len(shape))
+
+    tile = pl.BlockSpec((row_count, rank), lambda i: (i, 0))
+    copy_tile = pl.BlockSpec((row_count, width), lambda i: (i, 0))
+
+    def gathered_tile(m):
+        return pl.BlockSpec((1, 1, row_count, width), lambda i: (m, i, 0, 0))
+
+    return pl.pallas_call(
+        update_kernel,
+        grid=(n_fs,),
+        out_shape=(
+            *(jax.ShapeDtypeStruct(in_first.shape, f32),) * 4,
+            *(jax.ShapeDtypeStruct(in_master.shape, f32),) * 4,
+            *(jax.ShapeDtypeStruct((row_count * n_fs, width), bf16),) * 2,
+        ),
+        in_specs=[
+            fixed(dirs.shape),
+            fixed(moments_new.shape),
+            tile,
+            tile,
+            gathered_tile(0),
+            gathered_tile(1),
+            fixed(in_master.shape),
+            fixed(in_master.shape),
+        ],
+        out_specs=(
+            *(fixed(in_first.shape),) * 4,
+            *(fixed(in_master.shape),) * 4,
+            copy_tile,
+            copy_tile,
+        ),
+        scratch_shapes=[pltpu.VMEM((2, 2 * rank, width), bf16)],
+        compiler_params=pltpu.CompilerParams(vmem_limit_bytes=32 * 2**20),
+        name="update",
+    )(dirs, moments_new, in_basis, args[5], gathered, gathered, in_master, args[11])
+
+
+def fused_body(*args):
+    n_fs, n_tp = lax.axis_size("fs"), lax.axis_size("tp")
+    dirs, moments_new, gathered = exchange(n_fs, n_tp, *args)
+    return update(n_fs, dirs, moments_new, gathered, *args)
+
+
+def pick_body(*args):
+    n_fs, n_tp = lax.axis_size("fs"), lax.axis_size("tp")
+    first = args[6]
+    fits = n_fs % 2 == 0 and n_fs > 2 and n_tp > 1
+    if fits and first.shape[0] % 16 == 0 and first.shape[1] % 128 == 0:
+        return fused_body(*args)
+    return body(*args)
+
+
 def solution(mesh):
     return jax.shard_map(
-        body,
+        pick_body,
         mesh=mesh,
         in_specs=(
             P(("fs", "tp"), None),

time: 221 us -> 89.3 us (0.40)
  waiting for transfers between devices: 113 us -> 0 us
  Pallas kernels: 0 us -> 73.4 us
  blocking collectives: 69.4 us -> 0 us
  between operations: 15.9 us -> 0.68 us
  matrix products: 9.64 us -> 0 us
  local copies, waits for them, and re-layouts: 8.09 us -> 13.9 us
  other arithmetic: 4.47 us -> 0 us
    pallas_call x0 -> x2, Pallas kernels: none -> 73.4 us  [the longest x1 66.9 us: exchange(): pl.pallas_call(functools.partial(exchange_kernel, n_fs, n_tp), out_shape=...]
    all_gather x4 -> x0, blocking collectives: 59.2 us -> none  [the longest x1 15.9 us: body(): lax.all_gather(in_first, 'fs', axis=0, tiled=True)]
    all_gather x2 -> x0, waiting for transfers between devices: 52.3 us -> none  [the longest x1 30.6 us: body(): lax.all_gather(in_master_new.astype(jnp.bfloat16), 'fs', axis=0, tiled=True)]
    reduce_scatter x2 -> x0, waiting for transfers between devices: 44.6 us -> none  [the longest x1 31.4 us: body(): lax.psum_scatter(point_low, 'tp', scatter_dimension=1, tiled=True)]
    psum x1 -> x0, waiting for transfers between devices: 16.2 us -> none  [body(): sum_in, sum_point = lax.psum((part_in, part_point), 'fs')]
    psum x1 -> x0, blocking collectives: 10.2 us -> none  [body(): lax.psum(jnp.sum(sum_in * sum_in) + jnp.sum(sum_point * sum_point), 'tp')]
    dot_general x4 -> x0, matrix products: 9.64 us -> none  [the longest x2 5.07 us: weight_step(): jnp.dot(rows_here.astype(jnp.float32), direction, precision=lax.Precision...]
    unnamed x22 -> x26, local copies, waits for them, and re-layouts: 5.62 us -> 13.9 us
  transfers between devices with their start and end apart: 5 -> 0, of which waited for: 5 -> 0; matrix products, arithmetic and copies ran while one was open for 3% -> 0% of each run, Pallas kernels for 0% -> 0%
where the time goes in v1:
time: 89.3 us; the launch traced here: 88 us
  Pallas kernels  73.4 us (82%)
  local copies, waits for them, and re-layouts  13.9 us (16%)
    pallas_call x1, Pallas kernels, exchange(): pl.pallas_call(functools.partial(exchange_kernel, n_fs, n_tp), out_shape=...  66.9 us
    unnamed x26, local copies, waits for them, and re-layouts  13.9 us
    pallas_call x1, Pallas kernels, update(): pl.pallas_call(update_kernel, grid=(n_fs,), out_shape=(*(jax.ShapeDtypeSt...  6.49 us

profile of v1, /device:TPU:0, one launch (start us, length us, event | category | flops | bytes accessed | tf_op | source)
XLA Modules:
  0.0 88.0 jit_solution(15202535678271568777)
XLA Ops:
  0.6 0.0 copy-start.1
  0.7 1.0 %copy-done.1 = bf16[2048,128]{1,0:T(8,128)(2,1)S(1)} copy-done((bf16[2048,128]{1,0:T(8,128)(2,1)S(1)}, bf16[2048,128]{1,0:T(8,128)(2,1)}, u32[]{:S(2)}) %copy-start.1) | copy-done | bytes 524312
  1.7 0.0 copy-start.2
  1.7 1.0 %copy-done.2 = bf16[2048,128]{1,0:T(8,128)(2,1)S(1)} copy-done((bf16[2048,128]{1,0:T(8,128)(2,1)S(1)}, bf16[2048,128]{1,0:T(8,128)(2,1)}, u32[]{:S(2)}) %copy-start.2) | copy-done | bytes 524312
  2.7 0.0 copy-start.3
  2.7 1.0 %copy-done.3 = f32[256,512]{1,0:T(8,128)S(1)} copy-done((f32[256,512]{1,0:T(8,128)S(1)}, f32[256,512]{1,0:T(8,128)}, u32[]{:S(2)}) %copy-start.3) | copy-done | bytes 524312
  3.8 0.0 copy-start.4
  3.8 1.0 %copy-done.4 = f32[256,512]{1,0:T(8,128)S(1)} copy-done((f32[256,512]{1,0:T(8,128)S(1)}, f32[256,512]{1,0:T(8,128)}, u32[]{:S(2)}) %copy-start.4) | copy-done | bytes 524312
  4.8 0.0 copy-start.5
  4.8 1.1 %copy-done.5 = bf16[192,2048]{1,0:T(8,128)(2,1)S(1)} copy-done((bf16[192,2048]{1,0:T(8,128)(2,1)S(1)}, bf16[192,2048]{1,0:T(8,128)(2,1)}, u32[]{:S(2)}) %copy-start.5) | copy-done | bytes 786456
  6.0 0.0 copy-start.6
  6.0 1.1 %copy-done.6 = bf16[192,2048]{1,0:T(8,128)(2,1)S(1)} copy-done((bf16[192,2048]{1,0:T(8,128)(2,1)S(1)}, bf16[192,2048]{1,0:T(8,128)(2,1)}, u32[]{:S(2)}) %copy-start.6) | copy-done | bytes 786456
  7.1 0.0 copy-start.7
  7.1 1.1 %copy-done.7 = bf16[192,2048]{1,0:T(8,128)(2,1)S(1)} copy-done((bf16[192,2048]{1,0:T(8,128)(2,1)S(1)}, bf16[192,2048]{1,0:T(8,128)(2,1)}, u32[]{:S(2)}) %copy-start.7) | copy-done | bytes 786456
  8.2 0.0 copy-start.8
  8.2 1.1 %copy-done.8 = bf16[192,2048]{1,0:T(8,128)(2,1)S(1)} copy-done((bf16[192,2048]{1,0:T(8,128)(2,1)S(1)}, bf16[192,2048]{1,0:T(8,128)(2,1)}, u32[]{:S(2)}) %copy-start.8) | copy-done | bytes 786456
  9.4 0.0 copy-start.9
  9.4 0.8 copy-done.9
  10.1 0.0 copy-start.10
  10.1 0.8 copy-done.10
  10.9 0.0 copy-start.11
  10.9 0.8 copy-done.11
  11.6 0.0 copy-start.12
  11.6 0.8 copy-done.12
  12.4 66.9 %exchange.1 = (f32[8,2,16,512]{3,2,1,0:T(8,128)S(1)}, f32[4,16,512]{2,1,0:T(8,128)S(1)}, bf16[2,8,256,512]{3,2,1,0:T(8,128)(2,1)}) custom-call(bf16[192,2048]{1,0:T(8,128)(2,1)S(1)} %copy-done.5, bf16[192,2048]{1,0:T(8,128)(2,1)S(1)} %copy-done.6, bf16[192,2048]{1,0:T(8,128)(2,1)S(1)} %copy-done.7, bf16[192,2048]{1,0:T(8,128)(2,1)S(1)} %copy-done.8, ...), custom_call_target="tpu_custom_call" | custom-call | tf_op jit(solution)/shard_map/exchange/pallas_call | solution.py:376
  79.3 0.0 copy-start
  79.3 2.2 %copy-done = bf16[2,8,256,512]{3,2,1,0:T(8,128)(2,1)S(1)} copy-done((bf16[2,8,256,512]{3,2,1,0:T(8,128)(2,1)S(1)}, bf16[2,8,256,512]{3,2,1,0:T(8,128)(2,1)}, u32[]{:S(2)}) %copy-start) | copy-done | bytes 4194328
  81.5 6.5 %update.1 = (f32[16,512]{1,0:T(8,128)}, f32[16,512]{1,0:T(8,128)}, f32[16,512]{1,0:T(8,128)}, f32[16,512]{1,0:T(8,128)}, f32[256,512]{1,0:T(8,128)}, /*index=5*/...) custom-call(f32[8,2,16,512]{3,2,1,0:T(8,128)S(1)} %get-tuple-element, ...), custom_call_target="tpu_custom_call" | custom-call | tf_op jit(solution)/shard_map/update/pallas_call | solution.py:486
Async XLA Ops:
  0.6 1.0 %copy-start.1 = (bf16[2048,128]{1,0:T(8,128)(2,1)S(1)}, bf16[2048,128]{1,0:T(8,128)(2,1)}, u32[]{:S(2)}) copy-start(bf16[2048,128]{1,0:T(8,128)(2,1)} %in_basis.3) | copy-start | bytes 1572868
  1.7 1.0 %copy-start.2 = (bf16[2048,128]{1,0:T(8,128)(2,1)S(1)}, bf16[2048,128]{1,0:T(8,128)(2,1)}, u32[]{:S(2)}) copy-start(bf16[2048,128]{1,0:T(8,128)(2,1)} %point_basis.3) | copy-start | bytes 1572868
  2.7 1.0 %copy-start.3 = (f32[256,512]{1,0:T(8,128)S(1)}, f32[256,512]{1,0:T(8,128)}, u32[]{:S(2)}) copy-start(f32[256,512]{1,0:T(8,128)} %in_master.3) | copy-start | bytes 1572868
  3.8 1.0 %copy-start.4 = (f32[256,512]{1,0:T(8,128)S(1)}, f32[256,512]{1,0:T(8,128)}, u32[]{:S(2)}) copy-start(f32[256,512]{1,0:T(8,128)} %point_master.3) | copy-start | bytes 1572868
  4.8 1.1 %copy-start.5 = (bf16[192,2048]{1,0:T(8,128)(2,1)S(1)}, bf16[192,2048]{1,0:T(8,128)(2,1)}, u32[]{:S(2)}) copy-start(bf16[192,2048]{1,0:T(8,128)(2,1)} %in_saved.1) | copy-start | bytes 2359300
  6.0 1.1 %copy-start.6 = (bf16[192,2048]{1,0:T(8,128)(2,1)S(1)}, bf16[192,2048]{1,0:T(8,128)(2,1)}, u32[]{:S(2)}) copy-start(bf16[192,2048]{1,0:T(8,128)(2,1)} %in_cot.1) | copy-start | bytes 2359300
  7.1 1.1 %copy-start.7 = (bf16[192,2048]{1,0:T(8,128)(2,1)S(1)}, bf16[192,2048]{1,0:T(8,128)(2,1)}, u32[]{:S(2)}) copy-start(bf16[192,2048]{1,0:T(8,128)(2,1)} %point_saved.1) | copy-start | bytes 2359300
  8.2 1.1 %copy-start.8 = (bf16[192,2048]{1,0:T(8,128)(2,1)S(1)}, bf16[192,2048]{1,0:T(8,128)(2,1)}, u32[]{:S(2)}) copy-start(bf16[192,2048]{1,0:T(8,128)(2,1)} %point_cot.1) | copy-start | bytes 2359300
  9.4 0.8 copy-start.9
  10.1 0.8 copy-start.10
  10.9 0.8 copy-start.11
  11.6 0.8 copy-start.12
  79.3 2.2 %copy-start = (bf16[2,8,256,512]{3,2,1,0:T(8,128)(2,1)S(1)}, bf16[2,8,256,512]{3,2,1,0:T(8,128)(2,1)}, u32[]{:S(2)}) copy-start(bf16[2,8,256,512]{3,2,1,0:T(8,128)(2,1)} %get-tuple-element.15.in_gathered.point_gathered) | copy-start | bytes 12582916

commit v2 on v1

--- a/solution.py
+++ b/solution.py
@@ -95,6 +95,7 @@
 
 MESH = pl.DeviceIdType.MESH
 HBM = pl.BlockSpec(memory_space=pl.ANY)
+VMEM_BYTES = 67_043_328
 WHOLE = pl.BlockSpec(memory_space=pltpu.VMEM)
 
 
@@ -122,10 +123,12 @@
     master,
     part,
     mate,
+    tp_put,
     tp_got,
     fs_got,
     total,
     dirs,
+    old,
     gathered,
     scalars,
     load_sem,
@@ -176,6 +179,10 @@
         (point_basis, basis.at[1]),
         (point_saved, saved.at[1]),
         (point_cot, cot.at[1]),
+        (in_first, old.at[0]),
+        (in_second, old.at[1]),
+        (point_first, old.at[2]),
+        (point_second, old.at[3]),
     )
     for k, (src, dst) in enumerate(sources):
         copy = pltpu.make_async_copy(src, dst, load_sem.at[k])
@@ -189,57 +196,65 @@
         pl.semaphore_signal(barrier, inc=1, device_id=(f, at_tp(step)), device_id_type=MESH)
 
     sends = []
-    outs = []
-
-    def put_out(m, order, slot):
-        copy = pltpu.make_async_copy(
-            gathered.at[m, slot], gathered_out.at[m, slot], out_sem.at[m, order]
+
+    def out_copy(m, slot):
+        return pltpu.make_async_copy(
+            gathered.at[m, slot], gathered_out.at[m, slot], out_sem.at[m, slot]
         )
-        copy.start()
-        outs.append(copy)
-
-    def ring_send(step):
-        for m in range(2):
-            slot = 2 * at_z(-step if m == 0 else step) + core
-            copy = remote(
-                gathered.at[m, slot],
-                gathered.at[m, slot],
-                ring_sems,
-                (m, step),
-                (2 * at_z(1 if m == 0 else -1) + core, t),
-            )
-            copy.start()
-            sends.append(copy)
-
-    def mate_send(step):
-        for m in range(2):
-            slot = 2 * at_z(-step if m == 0 else step) + core
-            copy = remote(
-                gathered.at[m, slot], gathered.at[m, slot], ring_mate_sems, (m, step), (mate_f, t)
-            )
-            copy.start()
-            sends.append(copy)
-            put_out(m, step, slot)
-
-    def ring_wait(step):
-        for m in range(2):
-            slot = 2 * at_z(-step - 1 if m == 0 else step + 1) + core
-            remote(
-                gathered.at[m, slot], gathered.at[m, slot], ring_sems, (m, step), (f, t)
-            ).wait_recv()
-
-    def ring_advance(step):
-        ring_wait(step - 1)
-        if step < n_z - 1:
-            ring_send(step)
-        mate_send(step)
+
+    def mate_copy(m, slot, sem):
+        return remote(
+            gathered.at[m, slot], gathered.at[m, slot], ring_mate_sems, (m, sem), (mate_f, t)
+        )
+
+    def line_copy(d, m, step):
+        slot = 2 * (z - step if d == 0 else z + step) + core
+        to = z + 1 if d == 0 else z - 1
+        return remote(
+            gathered.at[m, slot], gathered.at[m, slot], ring_sems, (d, m, step), (2 * to + core, t)
+        )
+
+    def line_sends(d, step):
+        if d == 0:
+            return (z >= step) & (z + 1 < n_z)
+        return (z + step < n_z) & (z >= 1)
+
+    def line_start(m, step):
+        for d in range(2):
+
+            @pl.when(line_sends(d, step))
+            def start():
+                line_copy(d, m, step).start()
+
+    def line_relay(m, step):
+        for d in range(2):
+            owner = z - 1 - step if d == 0 else z + 1 + step
+
+            @pl.when((owner >= 0) & (owner < n_z))
+            def arrived():
+                slot = 2 * owner + core
+                remote(
+                    gathered.at[m, slot], gathered.at[m, slot], ring_sems, (d, m, step), (f, t)
+                ).wait_recv()
+                if step + 1 < n_z - 1:
+
+                    @pl.when(line_sends(d, step + 1))
+                    def onward():
+                        line_copy(d, m, step + 1).start()
+
+                mate_copy(m, slot, owner).start()
+                out_copy(m, slot).start()
 
     for m in range(2):
         loads[m].wait()
         gathered[m, f] = master[m].astype(jnp.bfloat16)
     pl.semaphore_wait(barrier, n_fs + n_tp - 2)
-    ring_send(0)
-    mate_send(0)
+    for m in range(2):
+        line_start(m, 0)
+    for m in range(2):
+        mate_copy(m, f, z).start()
+        out_copy(m, f).start()
+    relays = [(m, step) for step in range(n_z - 1) for m in range(2)]
 
     for m in range(2):
         for k in range(3):
@@ -264,14 +279,17 @@
         remote(mate.at[m], mate.at[m], mate_sems, (m,), (mate_f, t)).wait_recv()
         for step in range(1, n_tp + 1):
             to = at_tp(step) if step < n_tp else t
-            part[m, core, to] = part[m, core, to] + mate[m, to]
-            if step < n_tp:
+            value = part[m, core, to] + mate[m, to]
+            if step == n_tp:
+                part[m, core, to] = value
+            else:
+                tp_put[m, step - 1] = value.astype(jnp.bfloat16)
                 copy = remote(
-                    part.at[m, core, to], tp_got.at[m, step - 1], tp_sems, (m, step - 1), (f, to)
+                    tp_put.at[m, step - 1], tp_got.at[m, step - 1], tp_sems, (m, step - 1), (f, to)
                 )
                 copy.start()
                 sends.append(copy)
-    ring_advance(1)
+    line_relay(*relays[0])
 
     for m in range(2):
         for step in range(1, n_tp):
@@ -282,7 +300,7 @@
             to = at_z(step) if step < n_z else z
             value = part[m, core, t, to]
             for k in range(n_tp - 1):
-                value = value + tp_got[m, k, to]
+                value = value + tp_got[m, k, to].astype(jnp.float32)
             total[m, to] = value
             if step < n_z:
                 copy = remote(
@@ -294,6 +312,7 @@
                 )
                 copy.start()
                 sends.append(copy)
+    line_relay(*relays[1])
     grads = []
     for m in range(2):
         value = total[m, z]
@@ -319,15 +338,18 @@
             result = result + scalars[base + step]
         return result[0:1, 0:1]
 
+    line_relay(*relays[2])
     squares = jnp.sum(grads[0] * grads[0] + grads[1] * grads[1], keepdims=True)
     squares = add_scalars(squares, n_tp, 0, tp_scalar_sems, lambda step: (f, at_tp(step)))
     squares = add_scalars(squares, n_fs, n_tp, fs_scalar_sems, lambda step: (at_fs(step), t))
+    line_relay(*relays[3])
     entries = 2.0 * rows * n_fs * width * n_tp
     clip = jnp.minimum(1.0, 1.0 / jnp.sqrt(squares / entries + 1e-06))
 
-    old = ((in_first, in_second), (point_first, point_second))
-    for m in range(2):
-        first, second, direction = moments(old[m][0][...], old[m][1][...], clip * grads[m])
+    for copy in loads[8:]:
+        copy.wait()
+    for m in range(2):
+        first, second, direction = moments(old[2 * m], old[2 * m + 1], clip * grads[m])
         moments_out[2 * m] = first
         moments_out[2 * m + 1] = second
         dirs[f, m] = direction
@@ -349,22 +371,30 @@
         slot = 2 * at_z(-step) + core
         remote(dirs.at[slot], dirs.at[slot], dir_sems, (step - 1,), (f, t)).wait_recv()
         dir_mate(step)
-    for step in range(2, n_z):
-        ring_advance(step)
+    for m, step in relays[4:]:
+        line_relay(m, step)
     for step in range(n_z):
         slot = 2 * at_z(-step) + 1 - core
         remote(dirs.at[slot], dirs.at[slot], dir_mate_sems, (step,), (f, t)).wait_recv()
-        for m in range(2):
-            slot = 2 * at_z(-step if m == 0 else step) + 1 - core
-            remote(
-                gathered.at[m, slot], gathered.at[m, slot], ring_mate_sems, (m, step), (f, t)
-            ).wait_recv()
-            put_out(m, n_z + step, slot)
     dirs_out[...] = dirs[...]
+    for m in range(2):
+        for owner in range(n_z):
+            slot = 2 * owner + 1 - core
+            mate_copy(m, slot, owner).wait_recv()
+            out_copy(m, slot).start()
     for copy in sends:
         copy.wait_send()
-    for copy in outs:
-        copy.wait()
+    for m in range(2):
+        for owner in range(n_z):
+            mate_copy(m, 2 * owner + core, owner).wait_send()
+        for slot in range(n_fs):
+            out_copy(m, slot).wait()
+        for step in range(n_z - 1):
+            for d in range(2):
+
+                @pl.when(line_sends(d, step))
+                def sent():
+                    line_copy(d, m, step).wait_send()
 
 
 def exchange(n_fs, n_tp, *args):
@@ -380,7 +410,7 @@
             jax.ShapeDtypeStruct((4, rows, width), f32),
             jax.ShapeDtypeStruct((2, n_fs, *master.shape), bf16),
         ),
-        in_specs=[HBM] * 6 + [WHOLE] * 4 + [HBM] * 2,
+        in_specs=[HBM] * 12,
         out_specs=(WHOLE, WHOLE, HBM),
         scratch_shapes=[
             pltpu.VMEM((2, *saved.shape), bf16),
@@ -389,13 +419,15 @@
             pltpu.VMEM((2, *master.shape), f32),
             pltpu.VMEM((2, 2, n_tp, n_z, rows, width), f32),
             pltpu.VMEM((2, n_tp, n_z, rows, width), f32),
-            pltpu.VMEM((2, n_tp - 1, n_z, rows, width), f32),
+            pltpu.VMEM((2, n_tp - 1, n_z, rows, width), bf16),
+            pltpu.VMEM((2, n_tp - 1, n_z, rows, width), bf16),
             pltpu.VMEM((2, n_z - 1, rows, width), f32),
             pltpu.VMEM((2, n_z, rows, width), f32),
             pltpu.VMEM((n_fs, 2, rows, width), f32),
+            pltpu.VMEM((4, rows, width), f32),
             pltpu.VMEM((2, n_fs, *master.shape), bf16),
             pltpu.VMEM((n_tp + n_fs, 8, 128), f32),
-            dma((8,)),
+            dma((12,)),
             dma((2, n_fs)),
             dma((2, 2)),
             dma((2, 2, n_tp - 1)),
@@ -404,11 +436,11 @@
             dma((2, n_fs - 1)),
             dma((2, n_z - 1)),
             dma((2, n_z)),
-            dma((2, 2, n_z - 1)),
+            dma((2, 2, 2, n_z - 1)),
             dma((2, 2, n_z)),
         ],
         compiler_params=pltpu.CompilerParams(
-            collective_id=0, has_side_effects=True, vmem_limit_bytes=48 * 2**20
+            collective_id=0, has_side_effects=True, vmem_limit_bytes=VMEM_BYTES
         ),
         name="exchange",
     )(*args)
@@ -508,7 +540,7 @@
             copy_tile,
         ),
         scratch_shapes=[pltpu.VMEM((2, 2 * rank, width), bf16)],
-        compiler_params=pltpu.CompilerParams(vmem_limit_bytes=32 * 2**20),
+        compiler_params=pltpu.CompilerParams(vmem_limit_bytes=VMEM_BYTES),
         name="update",
     )(dirs, moments_new, in_basis, args[5], gathered, gathered, in_master, args[11])
 
@@ -522,7 +554,7 @@
 def pick_body(*args):
     n_fs, n_tp = lax.axis_size("fs"), lax.axis_size("tp")
     first = args[6]
-    fits = n_fs % 2 == 0 and n_fs > 2 and n_tp > 1
+    fits = n_fs % 2 == 0 and n_fs > 4 and n_tp > 1
     if fits and first.shape[0] % 16 == 0 and first.shape[1] % 128 == 0:
         return fused_body(*args)
     return body(*args)

time: 89.3 us -> 64.4 us (0.72); the launches traced: 88 us -> 64 us
  local copies, waits for them, and re-layouts: 13.9 us -> 0 us
  Pallas kernels: 73.4 us -> 63.4 us
    unnamed x26 -> x0, local copies, waits for them, and re-layouts: 13.9 us -> none
    pallas_call x1, Pallas kernels: 66.9 us -> 53.5 us  [exchange(): pl.pallas_call(functools.partial(exchange_kernel, n_fs, n_tp), out_shape=...]
    pallas_call x1, Pallas kernels: 6.49 us -> 9.88 us  [update(): pl.pallas_call(update_kernel, grid=(n_fs,), out_shape=(*(jax.ShapeDtypeSt...]
where the time goes in v2:
time: 64.4 us; the launch traced here: 64 us
  Pallas kernels  63.4 us (98%)
  between operations  0.65 us (1%)
    pallas_call x1, Pallas kernels, exchange(): pl.pallas_call(functools.partial(exchange_kernel, n_fs, n_tp), out_shape=...  53.5 us
    pallas_call x1, Pallas kernels, update(): pl.pallas_call(update_kernel, grid=(n_fs,), out_shape=(*(jax.ShapeDtypeSt...  9.88 us

profile of v2, /device:TPU:0, one launch (start us, length us, event | category | flops | bytes accessed | tf_op | source)
XLA Modules:
  0.0 64.0 jit_solution(8774586263367690155)
XLA Ops:
  0.6 53.5 %exchange.1 = (f32[8,2,16,512]{3,2,1,0:T(8,128)}, f32[4,16,512]{2,1,0:T(8,128)}, bf16[2,8,256,512]{3,2,1,0:T(8,128)(2,1)}) custom-call(bf16[192,2048]{1,0:T(8,128)(2,1)} %in_saved.1, bf16[192,2048]{1,0:T(8,128)(2,1)} %in_cot.1, bf16[192,2048]{1,0:T(8,128)(2,1)} %point_saved.1, bf16[192,2048]{1,0:T(8,128)(2,1)} %point_cot.1, bf16[2048,128]{1,0:T(8,128)(2,1)} %in_basis.3, ...), custom_call_target="tpu_custom_call" | custom-call | tf_op jit(solution)/shard_map/exchange/pallas_call | solution.py:406
  54.1 9.9 %update.1 = (f32[16,512]{1,0:T(8,128)}, f32[16,512]{1,0:T(8,128)}, f32[16,512]{1,0:T(8,128)}, f32[16,512]{1,0:T(8,128)}, f32[256,512]{1,0:T(8,128)}, /*index=5*/...) custom-call(f32[8,2,16,512]{3,2,1,0:T(8,128)} %get-tuple-element.13., ...), custom_call_target="tpu_custom_call" | custom-call | tf_op jit(solution)/shard_map/update/pallas_call | solution.py:518

commit v3 on v2

--- a/solution.py
+++ b/solution.py
@@ -352,7 +352,7 @@
         first, second, direction = moments(old[2 * m], old[2 * m + 1], clip * grads[m])
         moments_out[2 * m] = first
         moments_out[2 * m + 1] = second
-        dirs[f, m] = direction
+        dirs[f, m] = direction.astype(jnp.bfloat16)
     for step in range(1, n_z):
         copy = remote(
             dirs.at[f], dirs.at[f], dir_sems, (step - 1,), (2 * at_z(step) + core, t)
@@ -406,7 +406,7 @@
     return pl.pallas_call(
         functools.partial(exchange_kernel, n_fs, n_tp),
         out_shape=(
-            jax.ShapeDtypeStruct((n_fs, 2, rows, width), f32),
+            jax.ShapeDtypeStruct((n_fs, 2, rows, width), bf16),
             jax.ShapeDtypeStruct((4, rows, width), f32),
             jax.ShapeDtypeStruct((2, n_fs, *master.shape), bf16),
         ),
@@ -423,7 +423,7 @@
             pltpu.VMEM((2, n_tp - 1, n_z, rows, width), bf16),
             pltpu.VMEM((2, n_z - 1, rows, width), f32),
             pltpu.VMEM((2, n_z, rows, width), f32),
-            pltpu.VMEM((n_fs, 2, rows, width), f32),
+            pltpu.VMEM((n_fs, 2, rows, width), bf16),
             pltpu.VMEM((4, rows, width), f32),
             pltpu.VMEM((2, n_fs, *master.shape), bf16),
             pltpu.VMEM((n_tp + n_fs, 8, 128), f32),
@@ -465,19 +465,16 @@
     point_master_new,
     in_copy,
     point_copy,
-    split,
+    whole,
 ):
     i = pl.program_id(0)
     f = lax.axis_index("fs")
-    rank = split.shape[1] // 2
+    rank = whole.shape[1]
 
     @pl.when(i == 0)
     def first_tile():
         for m in range(2):
-            whole = dirs[:, m].reshape(rank, split.shape[2])
-            high = whole.astype(jnp.bfloat16)
-            split[m, :rank] = high
-            split[m, rank:] = (whole - high.astype(jnp.float32)).astype(jnp.bfloat16)
+            whole[m] = dirs[:, m].reshape(rank, whole.shape[2])
         for k, out in enumerate(
             (in_first_new, in_second_new, point_first_new, point_second_new)
         ):
@@ -488,8 +485,7 @@
         (point_basis, point_gathered, point_master, point_step, point_master_new, point_copy),
     )
     for m, (basis, gathered, master, step, master_new, copy) in enumerate(groups):
-        twice = jnp.concatenate([basis[...], basis[...]], axis=1)
-        move = -jnp.dot(twice, split[m], preferred_element_type=jnp.float32)
+        move = -jnp.dot(basis[...], whole[m], preferred_element_type=jnp.float32)
         copy[...] = (gathered[0, 0].astype(jnp.float32) + move).astype(jnp.bfloat16)
 
         @pl.when(i == f)
@@ -539,7 +535,7 @@
             copy_tile,
             copy_tile,
         ),
-        scratch_shapes=[pltpu.VMEM((2, 2 * rank, width), bf16)],
+        scratch_shapes=[pltpu.VMEM((2, rank, width), bf16)],
         compiler_params=pltpu.CompilerParams(vmem_limit_bytes=VMEM_BYTES),
         name="update",
     )(dirs, moments_new, in_basis, args[5], gathered, gathered, in_master, args[11])

time: 64.4 us -> 61.8 us (0.960)
  Pallas kernels: 63.4 us -> 60.8 us
    pallas_call x1, Pallas kernels: 53.5 us -> 51.2 us  [exchange(): pl.pallas_call(functools.partial(exchange_kernel, n_fs, n_tp), out_shape=...]
where the time goes in v3:
time: 61.8 us; the launch traced here: 61.5 us
  Pallas kernels  60.8 us (98%)
  between operations  0.65 us (1%)
    pallas_call x1, Pallas kernels, exchange(): pl.pallas_call(functools.partial(exchange_kernel, n_fs, n_tp), out_shape=...  51.2 us
    pallas_call x1, Pallas kernels, update(): pl.pallas_call(update_kernel, grid=(n_fs,), out_shape=(*(jax.ShapeDtypeSt...  9.61 us

profile of v3, /device:TPU:0, one launch (start us, length us, event | category | flops | bytes accessed | tf_op | source)
XLA Modules:
  0.0 61.5 jit_solution(12358777140648123352)
XLA Ops:
  0.6 51.2 %exchange.1 = (bf16[8,2,16,512]{3,2,1,0:T(8,128)(2,1)}, f32[4,16,512]{2,1,0:T(8,128)}, bf16[2,8,256,512]{3,2,1,0:T(8,128)(2,1)}) custom-call(bf16[192,2048]{1,0:T(8,128)(2,1)} %in_saved.1, bf16[192,2048]{1,0:T(8,128)(2,1)} %in_cot.1, bf16[192,2048]{1,0:T(8,128)(2,1)} %point_saved.1, bf16[192,2048]{1,0:T(8,128)(2,1)} %point_cot.1, ...), custom_call_target="tpu_custom_call" | custom-call | tf_op jit(solution)/shard_map/exchange/pallas_call | solution.py:406
  51.9 9.6 %update.1 = (f32[16,512]{1,0:T(8,128)}, f32[16,512]{1,0:T(8,128)}, f32[16,512]{1,0:T(8,128)}, f32[16,512]{1,0:T(8,128)}, f32[256,512]{1,0:T(8,128)}, /*index=5*/...) custom-call(bf16[8,2,16,512]{3,2,1,0:T(8,128)(2,1)} %get-tuple-eleme, ...), custom_call_target="tpu_custom_call" | custom-call | tf_op jit(solution)/shard_map/update/pallas_call | solution.py:514
